TPU v7x, 128 devices: a whole 4x4x4 slice. The times are simulated.
128 devices in a mesh: sp: 16 (over z, x), dp: 8 (over y, core).
Axes of the slice: x: 4, y: 4, z: 4, core: 2. Of those that a mesh axis runs over, the one named last changes fastest.
Arguments:
- queries: bfloat16 [8, 2048, 2048], P('dp', 'sp'), may hold values from -9 to 9
- keys: bfloat16 [8, 2048, 512], P('dp', 'sp'), may hold values from -9 to 9
- values: bfloat16 [8, 2048, 512], P('dp', 'sp'), may hold values from -6 to 6
- out_grad: bfloat16 [8, 2048, 2048], P('dp', 'sp'), may hold values from -24 to 24
- layer_in: bfloat16 [8, 2048, 4096], P('dp', 'sp'), may hold values from -0.09375 to 0.09375
- key_weight: bfloat16 [4096, 512], P('dp'), may hold values from -0.09375 to 0.09375
- value_weight: bfloat16 [4096, 512], P('dp'), may hold values from -0.09375 to 0.09375
- query_gain: float32 [128], replicated, may hold values from 0.64 to 6.04
- key_gain: float32 [128], replicated, may hold values from 0.64 to 6.04
Outputs:
- grad_query: bfloat16 [8, 2048, 2048], P('dp', 'sp')
- grad_in: bfloat16 [8, 2048, 4096], P('dp', 'sp')
- grad_key_weight: float32 [4096, 512], P('dp')
- grad_value_weight: float32 [4096, 512], P('dp')
All inputs are finite; a program needn't handle non-finite values.
Results may differ from a plain program's by a relative error of at most 0.018.
The roundings to bfloat16 on the way count: a program that leaves them out, or rounds other values in their place, can miss the bound.
Values may be sent and summed in bfloat16 or wider, within the bound.
A program may use at most 128 MiB of HBM per device.

v0:
```python
from functools import partial
import math
import jax
import jax.numpy as jnp
from jax import lax
from jax.sharding import PartitionSpec as P

HEADS = 16
KV_HEADS = 4
HEAD_DIM = 128
GRID_W = 64
epsilon = 1e-06
rope_base = 10000.0


def sent_together(arrays, axis, dim, along):
    widths = [a.shape[along] for a in arrays]
    both = jnp.concatenate(arrays, axis=along)
    result = lax.all_gather(both, axis, axis=dim, tiled=True)
    return tuple(jnp.split(result, [sum(widths[:k]) for k in range(1, len(widths))], axis=along))


def padded_to(lines, peers):
    spare = -len(lines) % peers
    return jnp.pad(lines, [(0, spare)] + [(0, 0)] * (lines.ndim - 1))


def copy_for_each(array, axis):
    peers = lax.axis_size(axis)
    return lax.all_to_all(
        jnp.broadcast_to(array[None], (peers, *array.shape)), axis, 0, 0, tiled=True
    )


def laid_out(parts, dim):
    dims = list(parts.shape[1:])
    dims[dim] *= parts.shape[0]
    return jnp.moveaxis(parts, 0, dim).reshape(dims)


def collect(array, axis, dim):
    parts = copy_for_each(array, axis)
    return laid_out(parts, dim)


def cut_along(array, dim, peers):
    before, after = (array.shape[:dim], array.shape[dim + 1 :])
    return jnp.moveaxis(array.reshape(*before, peers, -1, *after), dim, 0)


def sum_at_owner(array, axis, dim):
    peers = lax.axis_size(axis)
    parts = lax.all_to_all(cut_along(array, dim, peers), axis, 0, 0, tiled=True)
    return jnp.sum(parts.astype(jnp.float32), axis=0)


def nested_sum(array, axes):
    lines = array.reshape(-1, array.shape[-1])
    padded = padded_to(lines, lax.axis_size(axes))
    whole = collect(sum_at_owner(padded, axes, 0).astype(jnp.bfloat16), axes, 0)
    return lax.slice_in_dim(whole, 0, len(lines)).reshape(array.shape).astype(jnp.float32)


def norm_rotate(vector, gain_vec, row_index, col_index):
    scaled = (
        vector * lax.rsqrt(jnp.mean(vector * vector, axis=-1, keepdims=True) + epsilon) * gain_vec
    )
    quarter = vector.shape[-1] // 4
    inverse = rope_base ** (-jnp.arange(quarter, dtype=jnp.float32) / quarter)
    pieces = []
    for offset, position in ((0, row_index), (2 * quarter, col_index)):
        angles = position.astype(jnp.float32)[:, None] * inverse[None, :]
        cosine = jnp.cos(angles)
        sine_part = jnp.sin(angles)
        first_half = scaled[:, offset : offset + quarter]
        second_half = scaled[:, offset + quarter : offset + 2 * quarter]
        pieces.append(first_half * cosine - second_half * sine_part)
        pieces.append(first_half * sine_part + second_half * cosine)
    return jnp.concatenate(pieces, axis=1)


def contract_cols(left_side, right_side):
    return lax.dot_general(
        left_side, right_side, (((1,), (1,)), ((), ())), preferred_element_type=jnp.float32
    )


def contract_rows(left_side, right_side):
    return lax.dot_general(
        left_side, right_side, (((0,), (0,)), ((), ())), preferred_element_type=jnp.float32
    )


def head_grads(query_rows, grad_rows, key_rows, value_rows, query_gain, key_gain):
    length = query_rows.shape[0]
    block_rows = math.gcd(length, 512)
    positions = jnp.arange(length, dtype=jnp.int32)
    row_index = positions // GRID_W
    col_index = positions % GRID_W
    q_rot, q_back = jax.vjp(
        partial(norm_rotate, gain_vec=query_gain, row_index=row_index, col_index=col_index),
        query_rows.astype(jnp.float32),
    )
    k_rot, k_back = jax.vjp(
        partial(norm_rotate, gain_vec=key_gain, row_index=row_index, col_index=col_index),
        key_rows.astype(jnp.float32),
    )
    q_bf = q_rot.astype(jnp.bfloat16)
    k_bf = k_rot.astype(jnp.bfloat16)
    score_scale = q_rot.shape[-1] ** (-0.5)

    def one_block(accums, block_index):
        k_acc, v_acc = accums
        row_start = block_index * block_rows
        q_block = lax.dynamic_slice_in_dim(q_bf, row_start, block_rows, 0)
        g_block = lax.dynamic_slice_in_dim(grad_rows, row_start, block_rows, 0)
        scores = contract_cols(q_block, k_bf) * score_scale
        shifted = jnp.exp(scores - jnp.max(scores, axis=1, keepdims=True))
        attn_probs = shifted / jnp.sum(shifted, axis=1, keepdims=True)
        probs_b = attn_probs.astype(jnp.bfloat16)
        attn_out = jnp.dot(probs_b, value_rows, preferred_element_type=jnp.float32)
        row_delta = jnp.sum(g_block.astype(jnp.float32) * attn_out, axis=1, keepdims=True)
        grad_probs = contract_cols(g_block, value_rows)
        grad_scores = (attn_probs * (grad_probs - row_delta)).astype(jnp.bfloat16)
        q_grad = jnp.dot(grad_scores, k_bf, preferred_element_type=jnp.float32) * score_scale
        k_acc = k_acc + contract_rows(grad_scores, q_block) * score_scale
        v_acc = v_acc + contract_rows(probs_b, g_block)
        return ((k_acc, v_acc), q_grad)

    zeros_init = jnp.zeros(query_rows.shape, jnp.float32)
    (k_acc, v_acc), q_grads = lax.scan(
        one_block, (zeros_init, zeros_init), jnp.arange(length // block_rows, dtype=jnp.int32)
    )
    grad_rq = q_grads.reshape(length, query_rows.shape[1])
    grad_q = q_back(grad_rq)[0].astype(jnp.bfloat16)
    grad_k = k_back(k_acc)[0].astype(jnp.bfloat16)
    return (grad_q, grad_k, v_acc.astype(jnp.bfloat16))


def on_device(
    queries, keys, values, out_grad, layer_in, key_weight, value_weight, query_gain, key_gain
):
    seq_count, tokens_here, _ = queries.shape
    model_width = layer_in.shape[2]
    group_size = HEADS // KV_HEADS
    kv_width = KV_HEADS * HEAD_DIM
    key_full, value_full = sent_together((key_weight, value_weight), "dp", 0, 1)
    query_part = queries.reshape(seq_count, tokens_here, HEADS, HEAD_DIM)
    grad_part = out_grad.reshape(seq_count, tokens_here, HEADS, HEAD_DIM)
    shape_wide = (seq_count, tokens_here, KV_HEADS, group_size, HEAD_DIM)
    key_part = jnp.broadcast_to(
        keys.reshape(seq_count, tokens_here, KV_HEADS, 1, HEAD_DIM), shape_wide
    ).reshape(seq_count, tokens_here, HEADS, HEAD_DIM)
    value_part = jnp.broadcast_to(
        values.reshape(seq_count, tokens_here, KV_HEADS, 1, HEAD_DIM), shape_wide
    ).reshape(seq_count, tokens_here, HEADS, HEAD_DIM)
    bundle = jnp.concatenate([query_part, grad_part, key_part, value_part], axis=3)
    arrived = lax.all_to_all(bundle, "sp", split_axis=2, concat_axis=1, tiled=True)
    arrived_seqs, length, head_count, _ = arrived.shape
    flat_heads = arrived.transpose(0, 2, 1, 3).reshape(
        arrived_seqs * head_count, length, 4 * HEAD_DIM
    )

    def one_item(one_head):
        grad_q, grad_k, grad_v = head_grads(
            one_head[:, :HEAD_DIM],
            one_head[:, HEAD_DIM : 2 * HEAD_DIM],
            one_head[:, 2 * HEAD_DIM : 3 * HEAD_DIM],
            one_head[:, 3 * HEAD_DIM :],
            query_gain,
            key_gain,
        )
        return jnp.concatenate([grad_q, grad_k, grad_v], axis=1)

    all_grads = lax.map(one_item, flat_heads)
    head_out = all_grads.reshape(arrived_seqs, head_count, length, 3 * HEAD_DIM).transpose(
        0, 2, 1, 3
    )
    token_grads = lax.all_to_all(head_out, "sp", split_axis=1, concat_axis=2, tiled=True)
    grad_query = token_grads[:, :, :, :HEAD_DIM].reshape(seq_count, tokens_here, HEADS * HEAD_DIM)

    def grouped(array):
        summed = jnp.sum(
            array.reshape(seq_count * tokens_here, KV_HEADS, group_size, HEAD_DIM).astype(
                jnp.float32
            ),
            axis=2,
        )
        return summed.astype(jnp.bfloat16).reshape(seq_count * tokens_here, kv_width)

    kv_grad = jnp.concatenate(
        [
            grouped(token_grads[:, :, :, HEAD_DIM : 2 * HEAD_DIM]),
            grouped(token_grads[:, :, :, 2 * HEAD_DIM :]),
        ],
        axis=1,
    )
    both_weights = jnp.concatenate([key_full, value_full], axis=1)
    grad_flat = contract_cols(kv_grad, both_weights)
    grad_in = grad_flat.astype(jnp.bfloat16).reshape(seq_count, tokens_here, model_width)
    flat_in = layer_in.reshape(seq_count * tokens_here, model_width)
    partial_sum = lax.psum_scatter(
        contract_rows(flat_in, kv_grad).astype(jnp.bfloat16), "dp", scatter_dimension=0, tiled=True
    )
    weight_grad = nested_sum(partial_sum, "sp")
    return (grad_query, grad_in, weight_grad[:, :kv_width], weight_grad[:, kv_width:])


def solution(mesh):
    in_specs = (
        P("dp", "sp", None),
        P("dp", "sp", None),
        P("dp", "sp", None),
        P("dp", "sp", None),
        P("dp", "sp", None),
        P("dp", None),
        P("dp", None),
        P(),
        P(),
    )
    out_specs = (P("dp", "sp", None), P("dp", "sp", None), P("dp", None), P("dp", None))
    return jax.shard_map(
        on_device, mesh=mesh, in_specs=in_specs, out_specs=out_specs, check_vma=False
    )
```

profile of v0, /device:TPU:1, one launch (start us, length us, event | category | flops | bytes accessed | tf_op | source)
XLA Modules:
  0.0 371.3 jit_solution(12669012684862657344)
XLA Ops:
  9.3 2.0 copy.71
  11.4 2.0 copy.72
  15.0 2.6 copy.75
  17.6 8.4 %all-to-all-start = ((bf16[1,128,16,512]{3,1,0,2:T(8,128)(2,1)}), bf16[1,128,16,512]{3,1,0,2:T(8,128)(2,1)S(1)}, u32[]{:S(2)}, u32[]{:S(2)}) async-start(bf16[1,128,16,512]{3,1,0,2:T(8,128)(2,1)} %copy.75), calls=%async_computation | async-start | bytes 4194304 | tf_op jit(solution)/shard_map/all_to_all | solution.py:158
  26.1 30.8 %all-to-all-done = bf16[1,128,16,512]{3,1,0,2:T(8,128)(2,1)S(1)} async-done(((bf16[1,128,16,512]{3,1,0,2:T(8,128)(2,1)}), bf16[1,128,16,512]{3,1,0,2:T(8,128)(2,1)S(1)}, u32[]{:S(2)}, u32[]{:S(2)}) %all-to-all-start) | async-done | bytes 2097184 | tf_op jit(solution)/shard_map/all_to_all | solution.py:158
  58.3 2.5 fusion.93
  63.1 2.6 fusion.56
  67.9 77.8 %while.24 = (s32[]{:T(128)}, f32[2048,128]{1,0:T(8,128)}, f32[2048,128]{1,0:T(8,128)}, f32[4,512,128]{2,1,0:T(8,128)}, s32[4]{0:T(128)S(1)}, /*index=5*/bf16[204...) while((s32[]{:T(128)}, f32[2048,128]{1,0:T(8,128)}, ...), condition=%wide.region_6.7_spmd.clone, body=%wide.region_2.6_spmd.clone.sunk | while | flops 1625815552 | bytes 93731832 | solution.py:131
  70.9 2.7 fusion.133
  73.8 3.2 fusion.134
  77.2 1.8 multiply_convert_fusion.2
  79.0 2.8 fusion.135
  81.8 2.5 fusion.136
  84.3 1.8 convolution_add_fusion.2
  89.0 2.7 fusion.133
  91.9 3.2 fusion.134
  95.3 1.8 multiply_convert_fusion.2
  97.1 3.2 fusion.135
  100.3 2.5 fusion.136
  102.8 3.1 convolution_add_fusion.2
  108.9 2.7 fusion.133
  111.8 3.2 fusion.134
  115.2 1.8 multiply_convert_fusion.2
  117.0 3.2 fusion.135
  120.2 2.5 fusion.136
  122.7 3.1 convolution_add_fusion.2
  128.8 2.7 fusion.133
  131.7 3.2 fusion.134
  135.1 1.8 multiply_convert_fusion.2
  136.9 3.2 fusion.135
  140.1 2.5 fusion.136
  142.5 3.1 convolution_add_fusion.2
  145.7 4.9 %fusion.95 = (f32[2048,32]{1,0:T(8,128)}, f32[2048,32]{1,0:T(8,128)}, f32[2048,32]{1,0:T(8,128)}, f32[2048,32]{1,0:T(8,128)S(1)}) fusion(f32[2048,128]{1,0:T(8,128)} %bitcast.71), kind=kLoop, calls=%fused_computation.137 | loop fusion | bytes 2097152 | tf_op jit(solution)/shard_map/while/body/eval_jaxpr/transpose(jvp())/split | solution.py:79
  152.2 2.3 copy.106
  154.5 2.2 copy.107
  159.0 4.0 %fusion.63 = (f32[2048,32]{0,1:T(8,128)S(1)}, f32[2048,32]{0,1:T(8,128)S(1)}, f32[2048,32]{0,1:T(8,128)S(1)}, f32[2048,32]{0,1:T(8,128)S(1)}, f32[2048,32]{0,1:T...) fusion(f32[2048,32]{0,1:T(8,128)} %copy.107, f32[2048,32]{0,1:T(8,128)} %copy.108, ...), kind=kLoop, calls=%fused_computation.95 | loop fusion | flops 1966080 | bytes 4210816 | tf_op jit(solution)/shard_map/while/body/eval_jaxpr/transpose(jvp())/add_any | solution.py:77
  164.9 2.2 copy.85
  168.4 5.7 %copy.87 = bf16[1,2048,1,384]{3,2,0,1:T(2,128)(2,1)} copy(bf16[1,2048,1,384]{1,3,2,0:T(8,128)(2,1)S(1)} %maximum_bitcast_fusion) | data formatting | bytes 3145728 | tf_op jit(solution)/shard_map/transpose;reshape | solution.py:176
  174.6 34.5 %reduce.3 = bf16[2048,384]{1,0:T(8,128)(2,1)S(1)} reduce(bf16[2048,1,1,384]{3,2,1,0:T(2,128)(2,1)} %bitcast.72, bf16[]{:T(256)} %broadcast.219), dimensions={1,2}, to_apply=%bitcast.40.reduce_sub_computation | reduce | bytes 3145730
  210.5 25.3 %all_to_all.43 = bf16[16,2,24576]{2,1,0:T(2,128)(2,1)S(1)} all-to-all(bf16[16,2,24576]{2,1,0:T(2,128)(2,1)} %reshape.148), channel_id=1, replica_groups=mesh['sp'=16,'dp'=8] {'sp'}, dimensions={0} | all-to-all | bytes 3145728 | tf_op jit(solution)/shard_map/all_to_all | solution.py:179
  235.8 6.3 %reshape.149 = bf16[2048,1,1,384]{3,2,1,0:T(2,128)(2,1)} reshape(bf16[16,2,24576]{2,1,0:T(2,128)(2,1)S(1)} %all_to_all.43) | data formatting | bytes 3145728
  242.1 2.1 copy.100
  245.9 5.5 %convert_bitcast_fusion = bf16[4096,1024]{0,1:T(8,128)(2,1)} fusion(bf16[1,128,4096]{2,1,0:T(8,128)(2,1)S(1)} %copy-done, bf16[128,512]{0,1:T(8,128)(2,1)S(1)} %bitcast.86, bf16[128,512]{0,1:T(8,128)(2,1)S(1)} %bitcast.84), kind=kOutput, calls=%fused_computation.21 | convolution fusion | flops 1078460416 | bytes 9699328 | tf_op jit(solution)/shard_map/dot_general | solution.py:89
  253.8 49.0 %reduce-scatter.2.cloned.1.call-done = bf16[512,1024]{0,1:T(8,128)(2,1)} async-done(((bf16[4096,1024]{0,1:T(8,128)(2,1)}), bf16[512,1024]{0,1:T(8,128)(2,1)}) %reduce-scatter.2.cloned.1.call-update) | async-done | bytes 1048592 | tf_op jit(solution)/shard_map/reduce_scatter | solution.py:202
  304.3 22.3 %all_to_all.44 = bf16[16,32,1024]{2,1,0:T(8,128)(2,1)S(1)} all-to-all(bf16[16,32,1024]{2,1,0:T(8,128)(2,1)S(1)} %bitcast.76), channel_id=1, replica_groups=mesh['sp'=16,'dp'=8] {'sp'}, dimensions={0} | all-to-all | bytes 2097152 | tf_op jit(solution)/shard_map/all_to_all | solution.py:53
  327.9 3.9 %all-to-all-start.3 = ((bf16[16,32,1024]{2,1,0:T(8,128)(2,1)}), bf16[16,32,1024]{2,1,0:T(8,128)(2,1)S(1)}, u32[]{:S(2)}, u32[]{:S(2)}) async-start(bf16[16,32,1024]{2,1,0:T(8,128)(2,1)} %broadcast_in_dim.70), calls=%async_computation.4 | async-start | bytes 2097152 | tf_op jit(solution)/shard_map/all_to_all | solution.py:30
  333.1 22.3 %all-gather.2.cloned.1.call-done = bf16[4096,1024]{1,0:T(8,128)(2,1)} async-done(((bf16[512,1024]{1,0:T(8,128)(2,1)}), bf16[4096,1024]{1,0:T(8,128)(2,1)}) %all-gather.2.cloned.1.call-update) | async-done | bytes 8388624 | tf_op jit(solution)/shard_map/all_gather | solution.py:19
  355.4 7.2 %fusion.13 = bf16[1,128,4096]{2,1,0:T(8,128)(2,1)} fusion(bf16[4096,1024]{1,0:T(8,128)(2,1)} %all-gather.2.cloned.1.call-done, bf16[128,512]{0,1:T(8,128)(2,1)S(1)} %bitcast.87, bf16[128,512]{0,1:T(8,128)(2,1)S(1)} %bitcast.85), kind=kOutput, calls=%fused_computation.23 | convolution fusion | flops 1074790400 | bytes 9699328 | tf_op jit(solution)/shard_map/dot_general | solution.py:83
  (176 shorter events, 39.3 us)
Async XLA Ops:
  7.2 238.7 %copy-start = (bf16[1,128,4096]{2,1,0:T(8,128)(2,1)S(1)}, bf16[1,128,4096]{2,1,0:T(8,128)(2,1)}, u32[]{:S(2)}) copy-start(bf16[1,128,4096]{2,1,0:T(8,128)(2,1)} %param.15) | copy-start | bytes 3145732
  17.6 39.4 %all-to-all-start = ((bf16[1,128,16,512]{3,1,0,2:T(8,128)(2,1)}), bf16[1,128,16,512]{3,1,0,2:T(8,128)(2,1)S(1)}, u32[]{:S(2)}, u32[]{:S(2)}) async-start(bf16[1,128,16,512]{3,1,0,2:T(8,128)(2,1)} %copy.75), calls=%async_computation | async-start | bytes 4194304 | tf_op jit(solution)/shard_map/all_to_all | solution.py:158
  26.0 276.8 %reduce-scatter.2.cloned.1.call-start = ((), (), s32[]{:S(2)}) async-start(), calls=%async_computation.6 | async-start | bytes 9437184 | tf_op jit(solution)/shard_map/reduce_scatter | solution.py:202
  58.3 4.4 %copy-start.21 = (f32[128]{0:T(128)S(1)}, f32[128]{0:T(128)}, u32[]{:S(2)}) copy-start(f32[128]{0:T(128)} %param.19) | copy-start | bytes 1540
  61.1 4.6 %copy-start.8 = (bf16[2048,128]{0,1:T(8,128)(2,1)}, bf16[2048,128]{0,1:T(8,128)(2,1)S(1)}, u32[]{:S(2)}) copy-start(bf16[2048,128]{0,1:T(8,128)(2,1)S(1)} %copy.102) | copy-start | bytes 1572868
  62.5 3.2 copy-start.10
  67.9 3.0 copy-start.5
  67.9 3.0 copy-start.13
  67.9 5.7 %copy-start.15 = (bf16[2048,128]{1,0:T(8,128)(2,1)}, bf16[2048,128]{1,0:T(8,128)(2,1)S(1)}, u32[]{:S(2)}) copy-start(bf16[2048,128]{1,0:T(8,128)(2,1)S(1)} %get-tuple-element.348) | copy-start | bytes 1572868 | tf_op jit(solution)/shard_map/while/body/eval_jaxpr/while
  67.9 5.8 %copy-start.3 = (bf16[2048,128]{1,0:T(8,128)(2,1)}, bf16[2048,128]{1,0:T(8,128)(2,1)S(1)}, u32[]{:S(2)}) copy-start(bf16[2048,128]{1,0:T(8,128)(2,1)S(1)} %get-tuple-element.349) | copy-start | bytes 1572868 | tf_op jit(solution)/shard_map/while/body/eval_jaxpr/while
  73.8 3.5 copy-start.1
  79.0 5.2 %copy-start.2 = (f32[512,2048]{1,0:T(8,128)S(1)}, f32[512,2048]{1,0:T(8,128)}, u32[]{:S(2)}) copy-start(f32[512,2048]{1,0:T(8,128)} %fusion.133) | copy-start | bytes 12582916 | tf_op jit(solution)/shard_map/while/body/eval_jaxpr/while
  86.0 3.0 copy-start.5
  86.0 3.0 copy-start.13
  86.1 5.7 %copy-start.15 = (bf16[2048,128]{1,0:T(8,128)(2,1)}, bf16[2048,128]{1,0:T(8,128)(2,1)S(1)}, u32[]{:S(2)}) copy-start(bf16[2048,128]{1,0:T(8,128)(2,1)S(1)} %get-tuple-element.348) | copy-start | bytes 1572868 | tf_op jit(solution)/shard_map/while/body/eval_jaxpr/while
  86.1 5.8 %copy-start.3 = (bf16[2048,128]{1,0:T(8,128)(2,1)}, bf16[2048,128]{1,0:T(8,128)(2,1)S(1)}, u32[]{:S(2)}) copy-start(bf16[2048,128]{1,0:T(8,128)(2,1)S(1)} %get-tuple-element.349) | copy-start | bytes 1572868 | tf_op jit(solution)/shard_map/while/body/eval_jaxpr/while
  91.9 3.5 copy-start.1
  97.1 5.6 %copy-start.2 = (f32[512,2048]{1,0:T(8,128)S(1)}, f32[512,2048]{1,0:T(8,128)}, u32[]{:S(2)}) copy-start(f32[512,2048]{1,0:T(8,128)} %fusion.133) | copy-start | bytes 12582916 | tf_op jit(solution)/shard_map/while/body/eval_jaxpr/while
  102.8 3.1 copy-start.4
  102.8 3.1 copy-start.6
  102.8 3.1 copy-start.14
  102.8 3.1 copy-start.16
  105.9 3.0 copy-start.5
  105.9 3.0 copy-start.13
  105.9 5.7 %copy-start.15 = (bf16[2048,128]{1,0:T(8,128)(2,1)}, bf16[2048,128]{1,0:T(8,128)(2,1)S(1)}, u32[]{:S(2)}) copy-start(bf16[2048,128]{1,0:T(8,128)(2,1)S(1)} %get-tuple-element.348) | copy-start | bytes 1572868 | tf_op jit(solution)/shard_map/while/body/eval_jaxpr/while
  105.9 5.8 %copy-start.3 = (bf16[2048,128]{1,0:T(8,128)(2,1)}, bf16[2048,128]{1,0:T(8,128)(2,1)S(1)}, u32[]{:S(2)}) copy-start(bf16[2048,128]{1,0:T(8,128)(2,1)S(1)} %get-tuple-element.349) | copy-start | bytes 1572868 | tf_op jit(solution)/shard_map/while/body/eval_jaxpr/while
  111.8 3.5 copy-start.1
  117.0 5.6 %copy-start.2 = (f32[512,2048]{1,0:T(8,128)S(1)}, f32[512,2048]{1,0:T(8,128)}, u32[]{:S(2)}) copy-start(f32[512,2048]{1,0:T(8,128)} %fusion.133) | copy-start | bytes 12582916 | tf_op jit(solution)/shard_map/while/body/eval_jaxpr/while
  122.6 3.1 copy-start.4
  122.6 3.1 copy-start.6
  122.6 3.1 copy-start.14
  122.6 3.1 copy-start.16
  125.8 3.0 copy-start.5
  125.8 3.0 copy-start.13
  125.8 5.7 %copy-start.15 = (bf16[2048,128]{1,0:T(8,128)(2,1)}, bf16[2048,128]{1,0:T(8,128)(2,1)S(1)}, u32[]{:S(2)}) copy-start(bf16[2048,128]{1,0:T(8,128)(2,1)S(1)} %get-tuple-element.348) | copy-start | bytes 1572868 | tf_op jit(solution)/shard_map/while/body/eval_jaxpr/while
  125.8 5.8 %copy-start.3 = (bf16[2048,128]{1,0:T(8,128)(2,1)}, bf16[2048,128]{1,0:T(8,128)(2,1)S(1)}, u32[]{:S(2)}) copy-start(bf16[2048,128]{1,0:T(8,128)(2,1)S(1)} %get-tuple-element.349) | copy-start | bytes 1572868 | tf_op jit(solution)/shard_map/while/body/eval_jaxpr/while
  131.7 3.5 copy-start.1
  136.9 5.6 %copy-start.2 = (f32[512,2048]{1,0:T(8,128)S(1)}, f32[512,2048]{1,0:T(8,128)}, u32[]{:S(2)}) copy-start(f32[512,2048]{1,0:T(8,128)} %fusion.133) | copy-start | bytes 12582916 | tf_op jit(solution)/shard_map/while/body/eval_jaxpr/while
  142.5 3.1 copy-start.4
  142.5 3.1 copy-start.6
  142.5 3.1 copy-start.14
  142.5 3.1 copy-start.16
  150.6 7.1 %copy-start.7 = (f32[2048,128]{1,0:T(8,128)S(1)}, f32[2048,128]{1,0:T(8,128)}, u32[]{:S(2)}) copy-start(f32[2048,128]{1,0:T(8,128)} %get-tuple-element.69) | copy-start | bytes 3145732
  157.7 5.3 %copy-start.11 = (bf16[2048,128]{0,1:T(8,128)(2,1)S(1)}, bf16[2048,128]{0,1:T(8,128)(2,1)}, u32[]{:S(2)}) copy-start(bf16[2048,128]{0,1:T(8,128)(2,1)} %copy-done.10) | copy-start | bytes 1572868
  159.0 4.5 %copy-start.9 = (bf16[2048,128]{0,1:T(8,128)(2,1)S(1)}, bf16[2048,128]{0,1:T(8,128)(2,1)}, u32[]{:S(2)}) copy-start(bf16[2048,128]{0,1:T(8,128)(2,1)} %copy-done.8) | copy-start | bytes 1572868
  251.5 103.9 %all-gather.2.cloned.1.call-start = ((), (), s32[]{:S(2)}) async-start(), calls=%async_computation.5 | async-start | bytes 9437184 | tf_op jit(solution)/shard_map/all_gather | solution.py:19
  326.6 5.2 %copy-start.17 = (bf16[1,128,16,128]{3,1,2,0:T(8,128)(2,1)S(1)}, bf16[1,128,16,128]{3,1,2,0:T(8,128)(2,1)}, u32[]{:S(2)}) copy-start(bf16[1,128,16,128]{3,1,2,0:T(8,128)(2,1)} %get-tuple-element.217) | copy-start | bytes 1572868
  327.9 34.7 %all-to-all-start.3 = ((bf16[16,32,1024]{2,1,0:T(8,128)(2,1)}), bf16[16,32,1024]{2,1,0:T(8,128)(2,1)S(1)}, u32[]{:S(2)}, u32[]{:S(2)}) async-start(bf16[16,32,1024]{2,1,0:T(8,128)(2,1)} %broadcast_in_dim.70), calls=%async_computation.4 | async-start | bytes 2097152 | tf_op jit(solution)/shard_map/all_to_all | solution.py:30
  (8 other events, 12.7 us)
Sparse Core Ops, SparseCore 0:
  251.6 51.1 reduce-scatter.1
  305.1 50.2 all-gather.1
where the time goes:
time: 373 us; the launch traced here: 371 us
  waiting for transfers between devices  102 us (27%)
  matrix products  69.1 us (19%)
  other arithmetic  63.2 us (17%)
  local copies, waits for them, and re-layouts  59.7 us (16%)
  blocking collectives  47.5 us (13%)
  between operations  14.4 us (4%)
  starting transfers between devices  12.4 us (3%)
    reduce_scatter x1, waiting for transfers between devices, on_device(): lax.psum_scatter(contract_rows(flat_in, kv_grad).astype(jnp.bfloat16), 'd...  49 us
    unnamed x3, other arithmetic  34.5 us
    all_to_all x1, waiting for transfers between devices, on_device(): lax.all_to_all(bundle, 'sp', split_axis=2, concat_axis=1, tiled=True)  30.8 us
    dot_general x9, matrix products, contract_rows(): lax.dot_general(left_side, right_side, (((0,), (0,)), ((), ())), preferre...  28.9 us
    unnamed x38, local copies, waits for them, and re-layouts  27.8 us
    all_to_all x1, blocking collectives, on_device(): lax.all_to_all(head_out, 'sp', split_axis=1, concat_axis=2, tiled=True)  25.3 us
    all_to_all x1, blocking collectives, sum_at_owner(): parts = lax.all_to_all(cut_along(array, dim, peers), axis, 0, 0, tiled=True)  22.3 us
    all_gather x1, waiting for transfers between devices, sent_together(): result = lax.all_gather(both, axis, axis=dim, tiled=True)  22.3 us
  transfers between devices with their start and end apart: 4, of which 3 were waited for; matrix products, arithmetic and copies ran while one was open for 3% of the time, Pallas kernels for 0%

commit v1 on v0

--- a/solution.py
+++ b/solution.py
@@ -176,7 +176,10 @@
     head_out = all_grads.reshape(arrived_seqs, head_count, length, 3 * HEAD_DIM).transpose(
         0, 2, 1, 3
     )
-    token_grads = lax.all_to_all(head_out, "sp", split_axis=1, concat_axis=2, tiled=True)
+    token_grads = jnp.concatenate(
+        lax.all_to_all(jnp.stack(jnp.split(head_out, lax.axis_size("sp"), axis=1)), "sp", 0, 0),
+        axis=2,
+    )
     grad_query = token_grads[:, :, :, :HEAD_DIM].reshape(seq_count, tokens_here, HEADS * HEAD_DIM)
 
     def grouped(array):

time: 373 us -> 318 us (0.85)
  other arithmetic: 63.2 us -> 26.4 us
  local copies, waits for them, and re-layouts: 59.7 us -> 41.1 us
    unnamed x3 -> x2, other arithmetic: 34.5 us -> 0.01 us
    unnamed x38 -> x49, local copies, waits for them, and re-layouts: 27.8 us -> 17.5 us
    another operation x1, local copies, waits for them, and re-layouts: 5.66 us -> 0.05 us  [on_device(): jnp.stack(jnp.split(head_out, lax.axis_size('sp'), axis=1))]
  transfers between devices with their start and end apart: 4 -> 4, of which waited for: 3 -> 3; matrix products, arithmetic and copies ran while one was open for 3% -> 4% of each run, Pallas kernels for 0% -> 0%
where the time goes in v1:
time: 318 us; the launch traced here: 317 us
  waiting for transfers between devices  103 us (32%)
  matrix products  69.1 us (22%)
  blocking collectives  47.4 us (15%)
  local copies, waits for them, and re-layouts  41.1 us (13%)
  other arithmetic  26.4 us (8%)
  between operations  14.4 us (5%)
  starting transfers between devices  12.2 us (4%)
  loops' own time  3.3 us (1%)
    reduce_scatter x1, waiting for transfers between devices, on_device(): lax.psum_scatter(contract_rows(flat_in, kv_grad).astype(jnp.bfloat16), 'd...  49 us
    all_to_all x1, waiting for transfers between devices, on_device(): lax.all_to_all(bundle, 'sp', split_axis=2, concat_axis=1, tiled=True)  30.8 us
    dot_general x9, matrix products, contract_rows(): lax.dot_general(left_side, right_side, (((0,), (0,)), ((), ())), preferre...  28.9 us
    all_to_all x1, blocking collectives, on_device(): lax.all_to_all(jnp.stack(jnp.split(head_out, lax.axis_size('sp'), axis=1)...  25.1 us
    all_gather x1, waiting for transfers between devices, sent_together(): result = lax.all_gather(both, axis, axis=dim, tiled=True)  22.8 us
    all_to_all x1, blocking collectives, sum_at_owner(): parts = lax.all_to_all(cut_along(array, dim, peers), axis, 0, 0, tiled=True)  22.3 us
    dot_general x9, matrix products, contract_cols(): lax.dot_general(left_side, right_side, (((1,), (1,)), ((), ())), preferre...  17.6 us
    unnamed x49, local copies, waits for them, and re-layouts  17.5 us
  transfers between devices with their start and end apart: 4, of which 3 were waited for; matrix products, arithmetic and copies ran while one was open for 4% of the time, Pallas kernels for 0%

profile of v1, /device:TPU:1, one launch (start us, length us, event | category | flops | bytes accessed | tf_op | source)
XLA Modules:
  0.0 316.5 jit_solution(3671656724658698648)
XLA Ops:
  9.3 2.0 copy.41
  11.4 2.0 copy.42
  13.6 1.4 pad_maximum_fusion
  15.0 2.6 copy.45
  17.6 8.4 %all-to-all-start = ((bf16[1,128,16,512]{3,1,0,2:T(8,128)(2,1)}), bf16[1,128,16,512]{3,1,0,2:T(8,128)(2,1)S(1)}, u32[]{:S(2)}, u32[]{:S(2)}) async-start(bf16[1,128,16,512]{3,1,0,2:T(8,128)(2,1)} %copy.45), calls=%async_computation | async-start | bytes 4194304 | tf_op jit(solution)/shard_map/all_to_all | solution.py:158
  26.1 30.8 %all-to-all-done = bf16[1,128,16,512]{3,1,0,2:T(8,128)(2,1)S(1)} async-done(((bf16[1,128,16,512]{3,1,0,2:T(8,128)(2,1)}), bf16[1,128,16,512]{3,1,0,2:T(8,128)(2,1)S(1)}, u32[]{:S(2)}, u32[]{:S(2)}) %all-to-all-start) | async-done | bytes 2097184 | tf_op jit(solution)/shard_map/all_to_all | solution.py:158
  57.0 1.3 copy-done.12
  58.3 2.5 fusion.109
  63.1 2.6 fusion.56
  67.9 78.6 %while.24 = (s32[]{:T(128)}, f32[2048,128]{1,0:T(8,128)}, f32[2048,128]{1,0:T(8,128)}, f32[4,512,128]{2,1,0:T(8,128)}, s32[4]{0:T(128)S(1)}, /*index=5*/bf16[204...) while((s32[]{:T(128)}, f32[2048,128]{1,0:T(8,128)}, ...), condition=%wide.region_6.7_spmd.clone, body=%wide.region_2.6_spmd.clone.sunk | while | flops 1625815552 | bytes 93731832 | solution.py:131
  71.1 2.8 fusion.149
  74.0 3.2 %fusion.150 = f32[512]{0:T(512)S(1)} fusion(bf16[2048,128]{1,0:T(8,128)(2,1)S(1)} %get-tuple-element.310, f32[512,2048]{1,0:T(8,128)} %fusion.149, bf16[512,128]{0,1:T(8,128)(2,1)S(1)} %copy.79), kind=kOutput, calls=%fused_computation.12.clone.1 | convolution fusion | flops 269680128 | bytes 4851712 | tf_op jit(solution)/shard_map/while/body/eval_jaxpr/while/body/eval_jaxpr/dot_general | solution.py:121
  77.4 1.8 multiply_convert_fusion.2
  79.2 2.8 fusion.151
  82.0 2.5 fusion.152
  84.5 1.8 convolution_add_fusion.2
  89.4 2.8 fusion.149
  92.3 3.2 %fusion.150 = f32[512]{0:T(512)S(1)} fusion(bf16[2048,128]{1,0:T(8,128)(2,1)S(1)} %get-tuple-element.310, f32[512,2048]{1,0:T(8,128)} %fusion.149, bf16[512,128]{0,1:T(8,128)(2,1)S(1)} %copy.79), kind=kOutput, calls=%fused_computation.12.clone.1 | convolution fusion | flops 269680128 | bytes 4851712 | tf_op jit(solution)/shard_map/while/body/eval_jaxpr/while/body/eval_jaxpr/dot_general | solution.py:121
  95.8 1.8 multiply_convert_fusion.2
  97.5 3.2 fusion.151
  100.7 2.5 fusion.152
  103.2 3.1 convolution_add_fusion.2
  109.5 2.8 fusion.149
  112.4 3.2 %fusion.150 = f32[512]{0:T(512)S(1)} fusion(bf16[2048,128]{1,0:T(8,128)(2,1)S(1)} %get-tuple-element.310, f32[512,2048]{1,0:T(8,128)} %fusion.149, bf16[512,128]{0,1:T(8,128)(2,1)S(1)} %copy.79), kind=kOutput, calls=%fused_computation.12.clone.1 | convolution fusion | flops 269680128 | bytes 4851712 | tf_op jit(solution)/shard_map/while/body/eval_jaxpr/while/body/eval_jaxpr/dot_general | solution.py:121
  115.8 1.8 multiply_convert_fusion.2
  117.6 3.2 fusion.151
  120.8 2.5 fusion.152
  123.3 3.1 convolution_add_fusion.2
  129.6 2.8 fusion.149
  132.5 3.2 %fusion.150 = f32[512]{0:T(512)S(1)} fusion(bf16[2048,128]{1,0:T(8,128)(2,1)S(1)} %get-tuple-element.310, f32[512,2048]{1,0:T(8,128)} %fusion.149, bf16[512,128]{0,1:T(8,128)(2,1)S(1)} %copy.79), kind=kOutput, calls=%fused_computation.12.clone.1 | convolution fusion | flops 269680128 | bytes 4851712 | tf_op jit(solution)/shard_map/while/body/eval_jaxpr/while/body/eval_jaxpr/dot_general | solution.py:121
  135.9 1.8 multiply_convert_fusion.2
  137.7 3.2 fusion.151
  140.9 2.5 fusion.152
  143.4 3.1 convolution_add_fusion.2
  146.5 4.6 %fusion.111 = (f32[2048,32]{1,0:T(8,128)}, f32[2048,32]{1,0:T(8,128)}, f32[2048,32]{1,0:T(8,128)S(1)}, f32[2048,32]{1,0:T(8,128)S(1)}) fusion(f32[2048,128]{1,0:T(8,128)} %bitcast.131), kind=kLoop, calls=%fused_computation.169 | loop fusion | bytes 2097152 | tf_op jit(solution)/shard_map/while/body/eval_jaxpr/transpose(jvp())/split | solution.py:79
  151.4 2.3 copy.74
  153.7 2.2 copy.75
  157.3 3.7 %fusion.63 = (f32[2048,32]{0,1:T(8,128)S(1)}, f32[2048,32]{0,1:T(8,128)S(1)}, f32[2048,32]{0,1:T(8,128)S(1)}, f32[2048,32]{0,1:T(8,128)S(1)}, f32[2048,32]{0,1:T...) fusion(f32[2048,32]{0,1:T(8,128)} %copy.75, f32[2048,32]{0,1:T(8,128)} %copy.76, ...), kind=kLoop, calls=%fused_computation.95 | loop fusion | flops 1966080 | bytes 4210816 | tf_op jit(solution)/shard_map/while/body/eval_jaxpr/transpose(jvp())/add_any | solution.py:77
  162.7 1.4 copy.55
  164.9 25.1 %all_to_all.30 = bf16[16,1,128,1,384]{2,4,3,1,0:T(8,128)(2,1)S(1)} all-to-all(bf16[16,1,128,1,384]{2,4,3,1,0:T(8,128)(2,1)S(1)} %fusion.79), channel_id=1, replica_groups=mesh['sp'=16,'dp'=8] {'sp'}, dimensions={0} | all-to-all | bytes 3145728 | tf_op jit(solution)/shard_map/all_to_all | solution.py:180
  191.1 5.6 %convert_bitcast_fusion = bf16[4096,1024]{0,1:T(8,128)(2,1)} fusion(bf16[1,128,4096]{2,1,0:T(8,128)(2,1)S(1)} %copy-done, bf16[128,512]{0,1:T(8,128)(2,1)S(1)} %bitcast.144, bf16[128,512]{0,1:T(8,128)(2,1)S(1)} %bitcast.142), kind=kOutput, calls=%fused_computation.21 | convolution fusion | flops 1078460416 | bytes 9699328 | tf_op jit(solution)/shard_map/dot_general | solution.py:89
  199.0 49.0 %reduce-scatter.2.cloned.1.call-done = bf16[512,1024]{0,1:T(8,128)(2,1)} async-done(((bf16[4096,1024]{0,1:T(8,128)(2,1)}), bf16[512,1024]{0,1:T(8,128)(2,1)}) %reduce-scatter.2.cloned.1.call-update) | async-done | bytes 1048592 | tf_op jit(solution)/shard_map/reduce_scatter | solution.py:205
  248.0 1.5 copy.60
  249.5 22.3 %all_to_all.31 = bf16[16,32,1024]{2,1,0:T(8,128)(2,1)S(1)} all-to-all(bf16[16,32,1024]{2,1,0:T(8,128)(2,1)S(1)} %bitcast.134), channel_id=1, replica_groups=mesh['sp'=16,'dp'=8] {'sp'}, dimensions={0} | all-to-all | bytes 2097152 | tf_op jit(solution)/shard_map/all_to_all | solution.py:53
  273.1 3.7 %all-to-all-start.3 = ((bf16[16,32,1024]{2,1,0:T(8,128)(2,1)}), bf16[16,32,1024]{2,1,0:T(8,128)(2,1)S(1)}, u32[]{:S(2)}, u32[]{:S(2)}) async-start(bf16[16,32,1024]{2,1,0:T(8,128)(2,1)} %broadcast_in_dim.70), calls=%async_computation.4 | async-start | bytes 2097152 | tf_op jit(solution)/shard_map/all_to_all | solution.py:30
  277.8 22.8 %all-gather.2.cloned.1.call-done = bf16[4096,1024]{1,0:T(8,128)(2,1)} async-done(((bf16[512,1024]{1,0:T(8,128)(2,1)}), bf16[4096,1024]{1,0:T(8,128)(2,1)}) %all-gather.2.cloned.1.call-update) | async-done | bytes 8388624 | tf_op jit(solution)/shard_map/all_gather | solution.py:19
  300.6 7.3 %fusion.13 = bf16[1,128,4096]{2,1,0:T(8,128)(2,1)} fusion(bf16[4096,1024]{1,0:T(8,128)(2,1)} %all-gather.2.cloned.1.call-done, bf16[128,512]{0,1:T(8,128)(2,1)S(1)} %bitcast.145, bf16[128,512]{0,1:T(8,128)(2,1)S(1)} %bitcast.143), kind=kOutput, calls=%fused_computation.23 | convolution fusion | flops 1074790400 | bytes 9699328 | tf_op jit(solution)/shard_map/dot_general | solution.py:83
  308.2 1.5 fusion.108
  (183 shorter events, 28.1 us)
Async XLA Ops:
  7.2 184.0 %copy-start = (bf16[1,128,4096]{2,1,0:T(8,128)(2,1)S(1)}, bf16[1,128,4096]{2,1,0:T(8,128)(2,1)}, u32[]{:S(2)}) copy-start(bf16[1,128,4096]{2,1,0:T(8,128)(2,1)} %param.15) | copy-start | bytes 3145732
  17.6 39.4 %all-to-all-start = ((bf16[1,128,16,512]{3,1,0,2:T(8,128)(2,1)}), bf16[1,128,16,512]{3,1,0,2:T(8,128)(2,1)S(1)}, u32[]{:S(2)}, u32[]{:S(2)}) async-start(bf16[1,128,16,512]{3,1,0,2:T(8,128)(2,1)} %copy.45), calls=%async_computation | async-start | bytes 4194304 | tf_op jit(solution)/shard_map/all_to_all | solution.py:158
  26.0 222.0 %reduce-scatter.2.cloned.1.call-start = ((), (), s32[]{:S(2)}) async-start(), calls=%async_computation.6 | async-start | bytes 9437184 | tf_op jit(solution)/shard_map/reduce_scatter | solution.py:205
  60.8 1.8 copy-start.21
  61.1 2.0 copy-start.8
  61.1 1.8 copy-start.20
  62.5 3.2 copy-start.10
  67.9 2.3 copy-start.5
  67.9 2.3 copy-start.13
  67.9 5.9 %copy-start.15 = (bf16[2048,128]{1,0:T(8,128)(2,1)}, bf16[2048,128]{1,0:T(8,128)(2,1)S(1)}, u32[]{:S(2)}) copy-start(bf16[2048,128]{1,0:T(8,128)(2,1)S(1)} %get-tuple-element.309) | copy-start | bytes 1572868 | tf_op jit(solution)/shard_map/while/body/eval_jaxpr/while
  67.9 6.0 %copy-start.3 = (bf16[2048,128]{1,0:T(8,128)(2,1)}, bf16[2048,128]{1,0:T(8,128)(2,1)S(1)}, u32[]{:S(2)}) copy-start(bf16[2048,128]{1,0:T(8,128)(2,1)S(1)} %get-tuple-element.310) | copy-start | bytes 1572868 | tf_op jit(solution)/shard_map/while/body/eval_jaxpr/while
  74.0 3.5 %copy-start.1 = (f32[512,2048]{1,0:T(8,128)S(1)}, f32[512,2048]{1,0:T(8,128)}, u32[]{:S(2)}) copy-start(f32[512,2048]{1,0:T(8,128)} %fusion.149) | copy-start | bytes 12582916 | tf_op jit(solution)/shard_map/while/body/eval_jaxpr/while
  79.2 5.2 %copy-start.2 = (f32[512,2048]{1,0:T(8,128)S(1)}, f32[512,2048]{1,0:T(8,128)}, u32[]{:S(2)}) copy-start(f32[512,2048]{1,0:T(8,128)} %fusion.149) | copy-start | bytes 12582916 | tf_op jit(solution)/shard_map/while/body/eval_jaxpr/while
  86.2 2.3 copy-start.5
  86.3 2.3 copy-start.13
  86.3 5.9 %copy-start.15 = (bf16[2048,128]{1,0:T(8,128)(2,1)}, bf16[2048,128]{1,0:T(8,128)(2,1)S(1)}, u32[]{:S(2)}) copy-start(bf16[2048,128]{1,0:T(8,128)(2,1)S(1)} %get-tuple-element.309) | copy-start | bytes 1572868 | tf_op jit(solution)/shard_map/while/body/eval_jaxpr/while
  86.3 6.0 %copy-start.3 = (bf16[2048,128]{1,0:T(8,128)(2,1)}, bf16[2048,128]{1,0:T(8,128)(2,1)S(1)}, u32[]{:S(2)}) copy-start(bf16[2048,128]{1,0:T(8,128)(2,1)S(1)} %get-tuple-element.310) | copy-start | bytes 1572868 | tf_op jit(solution)/shard_map/while/body/eval_jaxpr/while
  92.3 3.5 %copy-start.1 = (f32[512,2048]{1,0:T(8,128)S(1)}, f32[512,2048]{1,0:T(8,128)}, u32[]{:S(2)}) copy-start(f32[512,2048]{1,0:T(8,128)} %fusion.149) | copy-start | bytes 12582916 | tf_op jit(solution)/shard_map/while/body/eval_jaxpr/while
  97.5 5.6 %copy-start.2 = (f32[512,2048]{1,0:T(8,128)S(1)}, f32[512,2048]{1,0:T(8,128)}, u32[]{:S(2)}) copy-start(f32[512,2048]{1,0:T(8,128)} %fusion.149) | copy-start | bytes 12582916 | tf_op jit(solution)/shard_map/while/body/eval_jaxpr/while
  103.2 3.1 copy-start.4
  103.2 3.1 copy-start.6
  103.2 3.1 copy-start.14
  103.2 3.1 copy-start.16
  106.3 2.3 copy-start.5
  106.3 2.3 copy-start.13
  106.4 5.9 %copy-start.15 = (bf16[2048,128]{1,0:T(8,128)(2,1)}, bf16[2048,128]{1,0:T(8,128)(2,1)S(1)}, u32[]{:S(2)}) copy-start(bf16[2048,128]{1,0:T(8,128)(2,1)S(1)} %get-tuple-element.309) | copy-start | bytes 1572868 | tf_op jit(solution)/shard_map/while/body/eval_jaxpr/while
  106.4 6.0 %copy-start.3 = (bf16[2048,128]{1,0:T(8,128)(2,1)}, bf16[2048,128]{1,0:T(8,128)(2,1)S(1)}, u32[]{:S(2)}) copy-start(bf16[2048,128]{1,0:T(8,128)(2,1)S(1)} %get-tuple-element.310) | copy-start | bytes 1572868 | tf_op jit(solution)/shard_map/while/body/eval_jaxpr/while
  112.4 3.5 %copy-start.1 = (f32[512,2048]{1,0:T(8,128)S(1)}, f32[512,2048]{1,0:T(8,128)}, u32[]{:S(2)}) copy-start(f32[512,2048]{1,0:T(8,128)} %fusion.149) | copy-start | bytes 12582916 | tf_op jit(solution)/shard_map/while/body/eval_jaxpr/while
  117.6 5.6 %copy-start.2 = (f32[512,2048]{1,0:T(8,128)S(1)}, f32[512,2048]{1,0:T(8,128)}, u32[]{:S(2)}) copy-start(f32[512,2048]{1,0:T(8,128)} %fusion.149) | copy-start | bytes 12582916 | tf_op jit(solution)/shard_map/while/body/eval_jaxpr/while
  123.3 3.1 copy-start.4
  123.3 3.1 copy-start.6
  123.3 3.1 copy-start.14
  123.3 3.1 copy-start.16
  126.4 2.3 copy-start.5
  126.4 2.3 copy-start.13
  126.4 5.9 %copy-start.15 = (bf16[2048,128]{1,0:T(8,128)(2,1)}, bf16[2048,128]{1,0:T(8,128)(2,1)S(1)}, u32[]{:S(2)}) copy-start(bf16[2048,128]{1,0:T(8,128)(2,1)S(1)} %get-tuple-element.309) | copy-start | bytes 1572868 | tf_op jit(solution)/shard_map/while/body/eval_jaxpr/while
  126.5 6.0 %copy-start.3 = (bf16[2048,128]{1,0:T(8,128)(2,1)}, bf16[2048,128]{1,0:T(8,128)(2,1)S(1)}, u32[]{:S(2)}) copy-start(bf16[2048,128]{1,0:T(8,128)(2,1)S(1)} %get-tuple-element.310) | copy-start | bytes 1572868 | tf_op jit(solution)/shard_map/while/body/eval_jaxpr/while
  132.5 3.5 %copy-start.1 = (f32[512,2048]{1,0:T(8,128)S(1)}, f32[512,2048]{1,0:T(8,128)}, u32[]{:S(2)}) copy-start(f32[512,2048]{1,0:T(8,128)} %fusion.149) | copy-start | bytes 12582916 | tf_op jit(solution)/shard_map/while/body/eval_jaxpr/while
  137.7 5.6 %copy-start.2 = (f32[512,2048]{1,0:T(8,128)S(1)}, f32[512,2048]{1,0:T(8,128)}, u32[]{:S(2)}) copy-start(f32[512,2048]{1,0:T(8,128)} %fusion.149) | copy-start | bytes 12582916 | tf_op jit(solution)/shard_map/while/body/eval_jaxpr/while
  143.3 3.1 copy-start.4
  143.3 3.1 copy-start.6
  143.4 3.1 copy-start.14
  143.4 3.1 copy-start.16
  151.4 5.6 %copy-start.7 = (f32[2048,128]{1,0:T(8,128)S(1)}, f32[2048,128]{1,0:T(8,128)}, u32[]{:S(2)}) copy-start(f32[2048,128]{1,0:T(8,128)} %get-tuple-element.69) | copy-start | bytes 3145732
  157.3 3.8 %copy-start.11 = (bf16[2048,128]{0,1:T(8,128)(2,1)S(1)}, bf16[2048,128]{0,1:T(8,128)(2,1)}, u32[]{:S(2)}) copy-start(bf16[2048,128]{0,1:T(8,128)(2,1)} %copy-done.10) | copy-start | bytes 1572868
  196.7 103.9 %all-gather.2.cloned.1.call-start = ((), (), s32[]{:S(2)}) async-start(), calls=%async_computation.5 | async-start | bytes 9437184 | tf_op jit(solution)/shard_map/all_gather | solution.py:19
  271.8 5.0 %copy-start.17 = (bf16[1,128,16,128]{1,3,2,0:T(8,128)(2,1)S(1)}, bf16[1,128,16,128]{1,3,2,0:T(8,128)(2,1)}, u32[]{:S(2)}) copy-start(bf16[1,128,16,128]{1,3,2,0:T(8,128)(2,1)} %get-tuple-element.178) | copy-start | bytes 1572868
  273.1 34.8 %all-to-all-start.3 = ((bf16[16,32,1024]{2,1,0:T(8,128)(2,1)}), bf16[16,32,1024]{2,1,0:T(8,128)(2,1)S(1)}, u32[]{:S(2)}, u32[]{:S(2)}) async-start(bf16[16,32,1024]{2,1,0:T(8,128)(2,1)} %broadcast_in_dim.70), calls=%async_computation.4 | async-start | bytes 2097152 | tf_op jit(solution)/shard_map/all_to_all | solution.py:30
  (8 other events, 11.7 us)
Sparse Core Ops, SparseCore 0:
  196.8 51.1 reduce-scatter.1
  250.3 50.2 all-gather.1
